TPU v7x, 32 devices: a whole 2x2x4 slice. The times are simulated.
32 devices in a mesh: grp: 2 (over y), fs: 4 (over z), tp: 4 (over x, core).
Axes of the slice: x: 2, y: 2, z: 4, core: 2. Of those that a mesh axis runs over, the one named last changes fastest.
Arguments:
- prompt_rows: bfloat16 [8192, 2048], P(('grp', 'fs')), parts along dimension 0, may hold values from -6 to 6
- up_master: float32 [2048, 8192], P('fs', 'tp'), may hold values from -0.125 to 0.125
- down_master: float32 [8192, 2048], P('fs', 'tp'), may hold values from -0.0625 to 0.0625
- norm_gain: float32 [2048], P('fs'), may hold values from 0.1 to 1.9
Outputs:
- up_sampler: bfloat16 [8, 2048, 2048], P(('grp', 'tp')), parts along dimension 0
- down_sampler: bfloat16 [8, 2048, 2048], P(('grp', 'tp')), parts along dimension 0
- layer_out: bfloat16 [8192, 2048], P(('grp', 'fs', 'tp')), parts along dimension 0
There are 2 independent parts, one for each index of `grp`. A program takes and returns all parts, laid end to end along the dimension named above; an argument that names none is the same for every part. Nothing has to cross between parts.
All inputs are finite; a program needn't handle non-finite values.
Results may differ from a plain program's by a relative error of at most 0.014.
Values may be sent and summed in bfloat16 or wider, within the bound.
A program may use at most 128 MiB of HBM per device.

v0:
```python
import functools

import jax
import jax.numpy as jnp
from jax import lax
from jax.experimental import pallas as pl
from jax.experimental.pallas import tpu as pltpu
from jax.sharding import PartitionSpec as P

eps = 1e-06
row_tile = 256
norm_tile = 64
copy_rows = 256
MESH = pl.DeviceIdType.MESH


def gather_kernel(
    n, tp, cuts, up_ref, down_ref, gain_ref, rows_ref, up_out, down_out, layer_out,
    up_all, down_all, normed, hidden, part, arrived,
    up_stage, down_stage, up_cast, down_cast, gain_tall, load_sem,
    local_sem, tp_send, tp_recv, z_send, z_recv, y_send, y_recv,
    sum_send, sum_recv, out_sem,
):
    y = lax.axis_index("grp")
    z = lax.axis_index("fs")
    me = lax.axis_index("tp")
    chips = tp // 2
    depths = (up_ref.shape[0], down_ref.shape[0] // tp)
    widths = (up_ref.shape[1] // tp, down_ref.shape[1])
    alls = (up_all, down_all)
    outs = (up_out, down_out)
    tokens = rows_ref.shape[0]
    share = tokens // tp

    def source(device, j):
        return lax.rem(device // 2 + j // 2, chips) * 2 + lax.rem(lax.rem(device, 2) + j % 2, 2)

    def target(j):
        return lax.rem(me // 2 + chips - j // 2, chips) * 2 + lax.rem(lax.rem(me, 2) + j % 2, 2)

    def columns(w, b, i=None):
        if i is None:
            return pl.ds(pl.multiple_of(b * widths[w], widths[w]), widths[w])
        width = widths[w] // cuts
        return pl.ds(pl.multiple_of(b * widths[w] + i * width, width), width)

    def block(w, a, b, h, i=None):
        half = depths[w] // 2
        first = a * depths[w] + h * half
        return alls[w].at[pl.ds(pl.multiple_of(first, half), half), columns(w, b, i)]

    def cast_block(w, t, first, count):
        if w == 0:
            return up_cast.at[pl.ds(pl.multiple_of(first, count), count), columns(0, t)]
        return down_cast.at[pl.ds(pl.multiple_of(t * depths[1] + first, count), count), :]

    def remote(src, dst, send, recv, device):
        return pltpu.make_async_remote_copy(
            src_ref=src, dst_ref=dst, send_sem=send, recv_sem=recv,
            device_id=device, device_id_type=MESH,
        )

    def tp_copy(w, j, k):
        h = y if k == 0 else 1 - y
        half = depths[w] // 2
        t = target(j)
        src = cast_block(w, t, h * half, half)
        return remote(src, block(w, z, me, h), tp_send.at[w, j, k], tp_recv.at[w, j, k], {"tp": t})

    def tp_arrival(w, j, k):
        h = y if k == 0 else 1 - y
        ref = block(w, z, source(me, j), h)
        return remote(ref, ref, tp_send.at[w, j, k], tp_recv.at[w, j, k], {"tp": target(j)})

    def z_copy(w, g, a, slot, device):
        ref = block(w, a, source(me, g // cuts), y, g % cuts)
        return remote(ref, ref, z_send.at[w, g, slot], z_recv.at[w, g, a], {"fs": device})

    def y_copy(w, g, a, h):
        ref = block(w, a, source(me, g // cuts), h, g % cuts)
        return remote(ref, ref, y_send.at[w, g, a], y_recv.at[w, g, a], {"grp": 1 - y})

    def local_copy(w, k):
        h = y if k == 0 else 1 - y
        half = depths[w] // 2
        src = cast_block(w, me, h * half, half)
        return pltpu.make_async_copy(src, block(w, z, me, h), local_sem.at[w, k])

    def out_copy(w, j):
        cols = columns(w, source(me, j))
        return pltpu.make_async_copy(alls[w].at[:, cols], outs[w].at[:, cols], out_sem.at[w, j])

    def sum_copy(j, k):
        t = target(k)
        cols = columns(1, source(me, j // cuts), j % cuts)
        src = part.at[pl.ds(pl.multiple_of(t * share, share), share), cols]
        return remote(src, arrived.at[k - 1, :, cols], sum_send.at[j, k], sum_recv.at[j, k], {"tp": t})

    def sum_arrival(j, k):
        cols = columns(1, source(source(me, k), j // cuts), j % cuts)
        ref = arrived.at[k - 1, :, cols]
        return remote(ref, ref, sum_send.at[j, k], sum_recv.at[j, k], {"tp": target(k)})

    def up_load(h, k):
        here = pl.ds(pl.multiple_of(h * (depths[0] // 2), depths[0] // 2), depths[0] // 2)
        return pltpu.make_async_copy(up_ref.at[here, :], up_stage.at[here, :], load_sem.at[k])

    down_load = pltpu.make_async_copy(down_ref, down_stage, load_sem.at[2])
    rows_load = pltpu.make_async_copy(rows_ref, normed, load_sem.at[3])
    up_load(y, 0).start()
    up_load(1 - y, 1).start()
    down_load.start()
    rows_load.start()
    barrier = pltpu.get_barrier_semaphore()
    for j in range(1, tp):
        pl.semaphore_signal(barrier, inc=1, device_id={"tp": target(j)}, device_id_type=MESH)
    pl.semaphore_signal(barrier, inc=1, device_id={"grp": 1 - y}, device_id_type=MESH)

    @pl.when(z > 0)
    def _():
        pl.semaphore_signal(barrier, inc=1, device_id={"fs": z - 1}, device_id_type=MESH)

    @pl.when(z < n - 1)
    def _():
        pl.semaphore_signal(barrier, inc=1, device_id={"fs": z + 1}, device_id_type=MESH)

    half = depths[0] // 2
    gain_tall[...] = jnp.broadcast_to(gain_ref[...], (128, depths[0])).T

    def cast_half(k):
        h = y if k == 0 else 1 - y
        up_load(h, k).wait()

        @pl.loop(0, half // norm_tile)
        def _(m):
            first = h * half + m * norm_tile
            here = pl.ds(pl.multiple_of(first, norm_tile), norm_tile)
            up_cast[here, :] = (up_stage[here, :] * gain_tall[here, :1]).astype(jnp.bfloat16)

    cast_half(0)
    local_copy(0, 0).start()
    pl.semaphore_wait(barrier, tp + (z + n - 1) // n + (2 * n - 2 - z) // n)

    def own_send(w, j):
        if j == 0:
            local_copy(w, 0).wait()
        elif j % cuts == 0:
            tp_arrival(w, j // cuts, 0).wait_recv()

        @pl.when(z < n - 1)
        def _():
            z_copy(w, j, z, z, z + 1).start()

        @pl.when(z > 0)
        def _():
            z_copy(w, j, z, n, z - 1).start()

    def process(w, j):
        for s in range(1, n):

            @pl.when(z - s >= 0)
            def _():
                a = z - s
                z_copy(w, j, a, a, z).wait_recv()

                @pl.when(z < n - 1)
                def _():
                    z_copy(w, j, a, a, z + 1).start()

                y_copy(w, j, a, y).start()

            @pl.when(z + s < n)
            def _():
                a = z + s
                z_copy(w, j, a, a, z).wait_recv()

                @pl.when(z > 0)
                def _():
                    z_copy(w, j, a, a, z - 1).start()

                y_copy(w, j, a, y).start()

    def finish(w, j):
        if j == 0:
            local_copy(w, 1).wait()
        elif j % cuts == 0:
            tp_arrival(w, j // cuts, 1).wait_recv()
        for a in range(n):

            @pl.when(z != a)
            def _():
                y_copy(w, j, a, 1 - y).wait_recv()

        cols = columns(w, source(me, j // cuts), j % cuts)
        if j % cuts == cuts - 1:
            out_copy(w, j // cuts).start()

        @pl.loop(0, tokens // row_tile)
        def _(m):
            here = pl.ds(pl.multiple_of(m * row_tile, row_tile), row_tile)
            if w == 0:
                acc = jnp.dot(normed[here, :], up_all[:, cols], preferred_element_type=jnp.float32)
                acc = jnp.maximum(acc, 0.0)
                hidden[here, cols] = (acc * acc).astype(jnp.bfloat16)
            else:
                acc = jnp.dot(hidden[here, :], down_all[:, cols], preferred_element_type=jnp.float32)
                part[here, cols] = acc.astype(jnp.bfloat16)

        if w == 1:
            for k in range(1, tp):
                sum_copy(j, k).start()

    def exchange(w, k):
        for j in range(1, tp):
            tp_copy(w, j, k).start()

    groups = [(w, j) for w in range(2) for j in range(tp * cuts)]
    exchange(0, 0)
    for g in range(cuts):
        own_send(*groups[g])
    cast_half(1)
    local_copy(0, 1).start()
    exchange(0, 1)
    down_load.wait()

    @pl.loop(0, down_ref.shape[0] // norm_tile)
    def _(m):
        here = pl.ds(pl.multiple_of(m * norm_tile, norm_tile), norm_tile)
        down_cast[here, :] = down_stage[here, :].astype(jnp.bfloat16)

    rows_load.wait()

    @pl.loop(0, tokens // norm_tile)
    def _(m):
        here = pl.ds(pl.multiple_of(m * norm_tile, norm_tile), norm_tile)
        values = normed[here, :].astype(jnp.float32)
        scale = lax.rsqrt(jnp.mean(values * values, axis=-1, keepdims=True) + eps)
        normed[here, :] = (values * scale).astype(jnp.bfloat16)

    exchange(1, 0)
    exchange(1, 1)
    local_copy(1, 0).start()
    local_copy(1, 1).start()
    ahead = 3
    for g in range(cuts, ahead):
        own_send(*groups[g])
    for g in range(len(groups)):
        process(*groups[g])
        if g + ahead < len(groups):
            own_send(*groups[g + ahead])
        if g >= 1:
            finish(*groups[g - 1])
    finish(*groups[-1])

    for j in range(tp * cuts):
        for k in range(1, tp):
            sum_arrival(j, k).wait_recv()

    @pl.loop(0, share // norm_tile)
    def _(m):
        here = pl.ds(pl.multiple_of(m * norm_tile, norm_tile), norm_tile)
        mine = pl.ds(pl.multiple_of(me * share + m * norm_tile, norm_tile), norm_tile)
        total = part[mine, :].astype(jnp.float32)
        for k in range(tp - 1):
            total = total + arrived[k, here, :].astype(jnp.float32)
        layer_out[here, :] = total.astype(jnp.bfloat16)

    for w in range(2):
        for j in range(tp):
            out_copy(w, j).wait()
            if j > 0:
                for k in range(2):
                    tp_copy(w, j, k).wait_send()
        for j in range(tp * cuts):

            @pl.when(z > 0)
            def _():
                z_copy(w, j, z, n, z - 1).wait_send()

            for a in range(n):

                @pl.when(jnp.logical_and(a <= z, z < n - 1))
                def _():
                    z_copy(w, j, a, a, z + 1).wait_send()

                @pl.when(jnp.logical_and(a > z, z > 0))
                def _():
                    z_copy(w, j, a, a, z - 1).wait_send()

                @pl.when(z != a)
                def _():
                    y_copy(w, j, a, y).wait_send()

    for j in range(tp * cuts):
        for k in range(1, tp):
            sum_copy(j, k).wait_send()


def place_kernel(up_in, down_in, layer_in, up_out, down_out, layer_out, *scratch):
    up_slots, down_slots, layer_slots, in_sem, out_sem = scratch
    arrays = (
        (up_in, up_slots, up_out),
        (down_in, down_slots, down_out),
        (layer_in, layer_slots, layer_out),
    )
    loads, stores = [], []
    for src, slots, dst in arrays:
        for first in range(0, src.shape[0], copy_rows):
            here = slice(first, min(first + copy_rows, src.shape[0]))
            i = len(loads)
            loads.append(pltpu.make_async_copy(src.at[here, :], slots.at[here, :], in_sem.at[i]))
            stores.append(pltpu.make_async_copy(slots.at[here, :], dst.at[here, :], out_sem.at[i]))
    for load in loads:
        load.start()
    for load, store in zip(loads, stores):
        load.wait()
        store.start()
    for store in stores:
        store.wait()


def on_device(prompt_rows, up_master, down_master, norm_gain):
    n = lax.axis_size("fs")
    tp = lax.axis_size("tp")
    bf16 = jnp.bfloat16
    up_rows, width = up_master.shape
    span = width // n
    fs_per_tp = n // tp
    up_width = fs_per_tp * span
    down_width = down_master.shape[1]
    if fs_per_tp > 1:
        up_master = up_master.reshape(up_rows, fs_per_tp, tp, span).swapaxes(1, 2)
        up_master = up_master.reshape(up_rows, width)
    cuts = 2 if up_width % 256 == 0 and down_width % 256 == 0 else 1
    tokens, model = prompt_rows.shape
    units = n * span
    share = tokens // tp
    vmem = pl.BlockSpec(memory_space=pltpu.VMEM)
    hbm = pl.BlockSpec(memory_space=pl.ANY)
    dma = pltpu.SemaphoreType.DMA
    up_shape = jax.ShapeDtypeStruct((model, units), bf16)
    down_shape = jax.ShapeDtypeStruct((units, model), bf16)
    up_all, down_all, layer_out = pl.pallas_call(
        functools.partial(gather_kernel, n, tp, cuts),
        out_shape=(up_shape, down_shape, jax.ShapeDtypeStruct((share, model), bf16)),
        in_specs=[hbm, hbm, vmem, hbm],
        out_specs=(hbm, hbm, vmem),
        scratch_shapes=[
            pltpu.VMEM((model, units), bf16),
            pltpu.VMEM((units, model), bf16),
            pltpu.VMEM((tokens, model), bf16),
            pltpu.VMEM((tokens, units), bf16),
            pltpu.VMEM((tokens, model), bf16),
            pltpu.VMEM((tp - 1, share, model), bf16),
            pltpu.VMEM(up_master.shape, jnp.float32),
            pltpu.VMEM(down_master.shape, jnp.float32),
            pltpu.VMEM(up_master.shape, bf16),
            pltpu.VMEM(down_master.shape, bf16),
            pltpu.VMEM((up_rows, 128), jnp.float32),
            dma((4,)),
            dma((2, 2)),
            dma((2, tp, 2)),
            dma((2, tp, 2)),
            dma((2, tp * cuts, n + 1)),
            dma((2, tp * cuts, n)),
            dma((2, tp * cuts, n)),
            dma((2, tp * cuts, n)),
            dma((tp * cuts, tp)),
            dma((tp * cuts, tp)),
            dma((2, tp)),
        ],
        compiler_params=pltpu.CompilerParams(
            collective_id=0, has_side_effects=True, vmem_limit_bytes=60 * 1024 * 1024
        ),
    )(up_master, down_master, norm_gain[None, :], prompt_rows)
    layer_shape = jax.ShapeDtypeStruct((share, model), bf16)
    moved = (up_shape, down_shape, layer_shape)
    jobs = sum(-(-shape.shape[0] // copy_rows) for shape in moved)
    up_sampler, down_sampler, layer_out = pl.pallas_call(
        place_kernel,
        out_shape=moved,
        in_specs=[hbm, hbm, hbm],
        out_specs=(hbm, hbm, hbm),
        scratch_shapes=[
            *(pltpu.VMEM(shape.shape, bf16) for shape in moved),
            dma((jobs,)),
            dma((jobs,)),
        ],
    )(up_all, down_all, layer_out)
    return (up_sampler[None], down_sampler[None], layer_out)


def solution(mesh):
    in_specs = (P(("grp", "fs"), None), P("fs", "tp"), P("fs", "tp"), P("fs"))
    out_specs = (
        P(("grp", "tp"), None, None),
        P(("grp", "tp"), None, None),
        P(("grp", "fs", "tp"), None),
    )
    return jax.shard_map(
        on_device, mesh=mesh, in_specs=in_specs, out_specs=out_specs, check_vma=False
    )
```

profile of v0, /device:TPU:1, one launch (start us, length us, event | category | flops | bytes accessed | tf_op | source)
XLA Modules:
  0.0 180.8 jit_solution(10552436475172593423)
XLA Ops:
  0.6 167.5 %shard_map.67 = (bf16[2048,2048]{1,0:T(8,128)(2,1)}, bf16[2048,2048]{1,0:T(8,128)(2,1)}, bf16[256,2048]{1,0:T(8,128)(2,1)}) custom-call(f32[512,2048]{1,0:T(8,128)} %up_ref.1, f32[2048,512]{1,0:T(8,128)} %down_ref.1, f32[1,512]{1,0:T(1,128)} %bitcast.3, bf16[1024,2048]{1,0:T(8,128)(2,1)} %rows_ref.1), custom_call_target="tpu_custom_call" | custom-call | tf_op jit(solution)/shard_map/pallas_call | solution.py:343
  168.1 12.7 %shard_map.68 = (bf16[2048,2048]{1,0:T(8,128)(2,1)}, bf16[2048,2048]{1,0:T(8,128)(2,1)}, bf16[256,2048]{1,0:T(8,128)(2,1)}) custom-call(bf16[2048,2048]{1,0:T(8,128)(2,1)} %get-tuple-element.9.up_in, bf16[2048,2048]{1,0:T(8,128)(2,1)} %get-tuple-element.10.down_in, bf16[256,2048]{1,0:T(8,128)(2,1)} %get-tuple-element.11.layer_in), custom_call_target="tpu_custom_call" | custom-call | tf_op jit(solution)/shard_map/pallas_call | solution.py:379
where the time goes:
time: 181 us
  Pallas kernels  180 us (99%)
    pallas_call x1, Pallas kernels, on_device(): pl.pallas_call(functools.partial(gather_kernel, n, tp, cuts), out_shape=(...  167 us
    pallas_call x1, Pallas kernels, on_device(): pl.pallas_call(place_kernel, out_shape=moved, in_specs=[hbm, hbm, hbm], o...  12.7 us

commit v1 on v0

v1 whole, which is shorter than its diff:
```python
import functools
import math

import jax
import jax.numpy as jnp
from jax import lax
from jax.experimental import pallas as pl
from jax.experimental.pallas import tpu as pltpu
from jax.sharding import PartitionSpec as P

eps = 1e-06
row_tile = 256
norm_tile = 64
pieces = 2
MESH = pl.DeviceIdType.MESH


def column_groups(tp, widths):
    groups = []
    for w in range(2):
        for j in range(tp):
            width = 256 if widths[w] % 256 == 0 else widths[w]
            if w == 1 and j == tp - 1 and width == 256:
                width = 128
            for first in range(0, widths[w], width):
                groups.append((w, j, first, width))
    return groups


def own_plan(count, steps, ahead, behind):
    plan, sent = [], ahead
    early, late = count * 2 // 9, count * 2 // 3
    for step in range(steps):
        if step < early:
            lead = ahead
        elif step >= late:
            lead = behind
        else:
            lead = round(ahead + (behind - ahead) * (step - early + 1) / (late - early + 1))
        now = []
        while sent < count and (sent <= step + lead or step == steps - 1):
            now.append(sent)
            sent += 1
        plan.append(now)
    return plan


def gather_kernel(
    n, tp, groups, up_ref, down_ref, gain_ref, rows_ref, up_all, down_all, part, arrived,
    normed, hidden, total, up_stage, down_stage, up_cast, down_cast, gain_tall, load_sem,
    tp_send, tp_recv, z_send, z_recv, y_send, y_recv, sum_send, sum_recv,
):
    y = lax.axis_index("grp")
    z = lax.axis_index("fs")
    me = lax.axis_index("tp")
    chips = tp // 2
    depths = (up_ref.shape[0], down_ref.shape[0] // tp)
    widths = (up_ref.shape[1] // tp, down_ref.shape[1])
    alls = (up_all, down_all)
    tokens = rows_ref.shape[0]
    share = tokens // tp
    count = len(groups)
    first_down = sum(group[0] == 0 for group in groups)
    twins = n > 2
    lag = max(n - 2, 2)
    steps = count + lag
    ahead, lead = 2, 3
    plan = own_plan(count, steps, ahead, -1)
    middle = jnp.logical_and(z > 0, z < n - 1)

    def source(device, j):
        return lax.rem(device // 2 + j // 2, chips) * 2 + lax.rem(lax.rem(device, 2) + j % 2, 2)

    def target(j):
        return lax.rem(me // 2 + chips - j // 2, chips) * 2 + lax.rem(lax.rem(me, 2) + j % 2, 2)

    far_first = [k for k in range(2, tp)] + [1]

    def columns(g, b):
        w, _, first, width = groups[g]
        return pl.ds(pl.multiple_of(b * widths[w] + first, math.gcd(width, 256)), width)

    def rows(w, a, h):
        half = depths[w] // 2
        return pl.ds(pl.multiple_of(a * depths[w] + h * half, half), half)

    def block(g, a, h):
        w, j, _, _ = groups[g]
        return alls[w].at[rows(w, a, h), columns(g, source(me, j))]

    def wide(w, b):
        return pl.ds(pl.multiple_of(b * widths[w], widths[w]), widths[w])

    def remote(src, dst, send, recv, device):
        return pltpu.make_async_remote_copy(
            src_ref=src, dst_ref=dst, send_sem=send, recv_sem=recv,
            device_id=device, device_id_type=MESH,
        )

    def half_of(k):
        return y if k == 0 else 1 - y

    def tp_copy(w, j, k):
        half = depths[w] // 2
        t = target(j)
        if w == 0:
            src = up_cast.at[pl.ds(pl.multiple_of(half_of(k) * half, half), half), wide(0, t)]
        else:
            src = down_cast.at[pl.ds(pl.multiple_of(t * depths[1] + half_of(k) * half, half), half), :]
        dst = alls[w].at[rows(w, z, half_of(k)), wide(w, me)]
        return remote(src, dst, tp_send.at[w], tp_recv.at[w, j - 1, k], {"tp": t})

    def tp_arrival(w, j, k):
        ref = alls[w].at[rows(w, z, half_of(k)), wide(w, source(me, j))]
        return remote(ref, ref, tp_send.at[w], tp_recv.at[w, j - 1, k], {"tp": target(j)})

    def in_pieces(g):
        return groups[g][0] == 1 and g >= count - pieces and depths[1] % 128 == 0

    def half_sem(g, a):
        return y_recv.at[count + (g - count + pieces) * n + a if in_pieces(g) else g]

    def z_copy(g, a, way, device):
        ref = block(g, a, y)
        slot = lax.rem(a - device + n, n) - 1
        return remote(ref, ref, z_send.at[way], z_recv.at[g, slot], {"fs": device})

    def own_up(g):
        return z_copy(g, z, 0, z + 1)

    def own_down(g):
        return z_copy(g, z, 1, z - 1)

    def twin_copy(g, a, device):
        ref = block(g, a, 1 - y)
        return remote(ref, ref, z_send.at[2], half_sem(g, a), {"fs": device})

    def y_copy(g, a, h):
        ref = block(g, a, h)
        return remote(ref, ref, y_send.at[0], half_sem(g, a), {"grp": 1 - y})

    def sum_copy(g, k):
        t = target(k)
        cols = columns(g, source(me, groups[g][1]))
        src = part.at[pl.ds(pl.multiple_of(t * share, share), share), cols]
        return remote(src, arrived.at[k - 1, :, cols], sum_send.at[0], sum_recv.at[0], {"tp": t})

    def up_load(j):
        half = depths[0] // 2
        here = pl.ds(pl.multiple_of(y * half, half), half)
        cols = wide(0, target(j))
        return pltpu.make_async_copy(up_ref.at[here, cols], up_stage.at[here, cols], load_sem.at[j])

    def late_load():
        half = depths[0] // 2
        here = pl.ds(pl.multiple_of((1 - y) * half, half), half)
        return pltpu.make_async_copy(up_ref.at[here, :], up_stage.at[here, :], load_sem.at[tp])

    down_load = pltpu.make_async_copy(down_ref, down_stage, load_sem.at[tp + 1])
    rows_load = pltpu.make_async_copy(rows_ref, normed, load_sem.at[tp + 2])
    order = [0] + far_first
    for j in order:
        up_load(j).start()
    late_load().start()
    rows_load.start()
    down_load.start()
    barrier = pltpu.get_barrier_semaphore()
    for j in range(1, tp):
        pl.semaphore_signal(barrier, inc=1, device_id={"tp": target(j)}, device_id_type=MESH)
    pl.semaphore_signal(barrier, inc=1, device_id={"grp": 1 - y}, device_id_type=MESH)

    @pl.when(z > 0)
    def _():
        pl.semaphore_signal(barrier, inc=1, device_id={"fs": z - 1}, device_id_type=MESH)

    @pl.when(z < n - 1)
    def _():
        pl.semaphore_signal(barrier, inc=1, device_id={"fs": z + 1}, device_id_type=MESH)

    gain_tall[...] = jnp.broadcast_to(gain_ref[...], (128, depths[0])).T

    def cast_up(j, k):
        half = depths[0] // 2
        tile = math.gcd(half, norm_tile)
        cols = wide(0, target(j))

        @pl.loop(0, half // tile)
        def _(m):
            first = pl.multiple_of(half_of(k) * half + m * tile, tile)
            here = pl.ds(first, tile)
            value = (up_stage[here, cols] * gain_tall[here, :1]).astype(jnp.bfloat16)
            if j == 0:
                up_all[pl.ds(pl.multiple_of(z * depths[0] + first, tile), tile), cols] = value
            else:
                up_cast[here, cols] = value

    def cast_down():
        tile = math.gcd(depths[1], norm_tile)

        @pl.loop(0, down_ref.shape[0] // tile)
        def _(m):
            here = pl.ds(pl.multiple_of(m * tile, tile), tile)
            down_cast[here, :] = down_stage[here, :].astype(jnp.bfloat16)

        @pl.loop(0, depths[1] // tile)
        def _(m):
            here = pl.ds(pl.multiple_of(me * depths[1] + m * tile, tile), tile)
            there = pl.ds(pl.multiple_of(z * depths[1] + m * tile, tile), tile)
            down_all[there, wide(1, me)] = down_stage[here, :].astype(jnp.bfloat16)

    def norm_rows(first, many):
        @pl.loop(0, many // norm_tile)
        def _(m):
            here = pl.ds(pl.multiple_of(first + m * norm_tile, norm_tile), norm_tile)
            values = normed[here, :].astype(jnp.float32)
            scale = lax.rsqrt(jnp.mean(values * values, axis=-1, keepdims=True) + eps)
            normed[here, :] = (values * scale).astype(jnp.bfloat16)

    def late_own(g):
        @pl.when(z == 1)
        def _():
            own_down(g).start()

        @pl.when(z == n - 2)
        def _():
            own_up(g).start()

    def early_own(g):
        w, j, first, _ = groups[g]
        if j > 0 and first == 0:
            tp_arrival(w, j, 0).wait_recv()

        @pl.when(z > 1)
        def _():
            own_down(g).start()

        @pl.when(z < n - 2)
        def _():
            own_up(g).start()

    def twin_own(g):
        w, j, first, _ = groups[g]
        if j > 0 and first == 0:
            tp_arrival(w, j, 1).wait_recv()
        if twins:
            for edge, near in ((0, 1), (n - 1, n - 2)):

                @pl.when(z == edge)
                def _():
                    twin_copy(g, edge, near).start()

    def at_edge(body):
        for edge, way in ((0, 1), (n - 1, -1)):

            @pl.when(z == edge)
            def _():
                body(lambda s: edge + way * s)

    def edge_receive(g, a):
        z_copy(g, a, 0, z).wait_recv()
        y_copy(g, a, y).start()

    def receive(step):
        @pl.when(middle)
        def _():
            for s in range(1, n - 1):
                g = step - (s - 1)
                if not 0 <= g < count:
                    continue

                @pl.when(z >= s)
                def _():
                    a = z - s
                    z_copy(g, a, 0, z).wait_recv()
                    z_copy(g, a, 0, z + 1).start()
                    if s == 1 and twins:

                        @pl.when(a != 0)
                        def _():
                            y_copy(g, a, y).start()
                    else:
                        y_copy(g, a, y).start()

                @pl.when(z + s < n)
                def _():
                    a = z + s
                    z_copy(g, a, 0, z).wait_recv()
                    z_copy(g, a, 1, z - 1).start()
                    if s == 1 and twins:

                        @pl.when(a != n - 1)
                        def _():
                            y_copy(g, a, y).start()
                    else:
                        y_copy(g, a, y).start()

        def edge(at):
            for s in range(2, n):
                g = step - (s - 2)
                if 0 <= g < count:
                    edge_receive(g, at(s))
            for g in plan[step]:
                edge_receive(g, at(1))

        at_edge(edge)

    def other_half(g, a):
        y_copy(g, a, 1 - y).wait_recv()

    def other_halves(g):
        w = groups[g][0]
        half = depths[w] // 2
        ref = alls[w].at[pl.ds(0, (n - 1) * half), columns(g, source(me, groups[g][1]))]
        remote(ref, ref, y_send.at[0], y_recv.at[g], {"grp": 1 - y}).wait_recv()

    def finish(g):
        w, j, _, width = groups[g]
        cols = columns(g, source(me, j))

        def product(a, fresh):
            deep = pl.ds(pl.multiple_of(a * depths[1], depths[1]), depths[1])

            @pl.loop(0, tokens // row_tile)
            def _(m):
                here = pl.ds(pl.multiple_of(m * row_tile, row_tile), row_tile)
                acc = jnp.dot(hidden[here, deep], down_all[deep, cols], preferred_element_type=jnp.float32)
                total[here, :] = acc if fresh else total[here, :] + acc

        if in_pieces(g):
            product(z, True)
            for s in range(1, n):
                for a in range(n):
                    if a - s < 0 and a + s > n - 1:
                        continue
                    near = z - a == s if a + s < n else a - z == s
                    if a + s < n and a - s >= 0:
                        near = jnp.logical_or(z - a == s, a - z == s)

                    @pl.when(near)
                    def _():
                        other_half(g, a)
                        product(a, False)

            @pl.loop(0, tokens // row_tile)
            def _(m):
                here = pl.ds(pl.multiple_of(m * row_tile, row_tile), row_tile)
                part[here, cols] = total[here, :].astype(jnp.bfloat16)
        else:
            other_halves(g)

            @pl.loop(0, tokens // row_tile)
            def _(m):
                here = pl.ds(pl.multiple_of(m * row_tile, row_tile), row_tile)
                if w == 0:
                    acc = jnp.dot(normed[here, :], up_all[:, cols], preferred_element_type=jnp.float32)
                    acc = jnp.maximum(acc, 0.0)
                    hidden[here, cols] = (acc * acc).astype(jnp.bfloat16)
                else:
                    acc = jnp.dot(hidden[here, :], down_all[:, cols], preferred_element_type=jnp.float32)
                    part[here, cols] = acc.astype(jnp.bfloat16)

        if w == 1:
            for k in far_first:
                sum_copy(g, k).start()

    up_load(0).wait()
    cast_up(0, 0)
    pl.semaphore_wait(barrier, tp + (z + n - 1) // n + (2 * n - 2 - z) // n)
    for g in range(ahead):
        early_own(g)
        late_own(g)
    for j in far_first:
        up_load(j).wait()
        cast_up(j, 0)
        tp_copy(0, j, 0).start()
    late_load().wait()
    for j in far_first + [0]:
        cast_up(j, 1)
        if j > 0:
            tp_copy(0, j, 1).start()
    rows_load.wait()
    quarter = tokens // 4

    def down_work():
        down_load.wait()
        cast_down()
        for k in range(2):
            for j in far_first:
                tp_copy(1, j, k).start()

    work = [functools.partial(norm_rows, i * quarter, quarter) for i in range(4)] + [down_work]
    for g in range(ahead):
        at_edge(lambda at: edge_receive(g, at(1)))
        work.pop(0)()
    sent = ahead
    for step in range(steps):
        receive(step)
        while sent < count and sent <= step + lead:
            early_own(sent)
            sent += 1
        for g in plan[step]:
            late_own(g)
        if step < count:
            twin_own(step)
        if work:
            work.pop(0)()
        if step >= lag:
            while work:
                work.pop(0)()
            finish(step - lag)

    def await_sends(ref, sem):
        remote(ref, ref, sem, sum_recv.at[0], {"grp": 1 - y}).wait_send()

    await_sends(up_cast.at[:, pl.ds(0, (tp - 1) * widths[0])], tp_send.at[0])
    await_sends(down_cast.at[pl.ds(0, (tp - 1) * depths[1]), :], tp_send.at[1])
    for edge in range(n):
        passed = n - 1 - (twins and edge == 1) - (twins and edge == n - 2)
        waits = [
            (z_send.at[0], edge + 1 if edge < n - 1 else 0),
            (z_send.at[1], n - edge if edge > 0 else 0),
            (z_send.at[2], int(twins and edge in (0, n - 1))),
            (y_send.at[0], passed),
        ]

        @pl.when(z == edge)
        def _():
            for sem, blocks in waits:
                if blocks:
                    await_sends(up_all.at[pl.ds(0, blocks * depths[0]), :], sem)

    remote(arrived, arrived, sum_send.at[0], sum_recv.at[0], {"grp": 1 - y}).wait()


def place_kernel(tp, up_in, down_in, part, arrived, up_out, down_out, layer_out, layer, sem):
    share = layer.shape[0]
    me = lax.axis_index("tp")
    copies = [
        pltpu.make_async_copy(src, dst, sem.at[i])
        for i, (src, dst) in enumerate(((up_in, up_out), (down_in, down_out), (layer, layer_out)))
    ]
    copies[0].start()
    copies[1].start()

    @pl.loop(0, share // norm_tile)
    def _(m):
        here = pl.ds(pl.multiple_of(m * norm_tile, norm_tile), norm_tile)
        mine = pl.ds(pl.multiple_of(me * share + m * norm_tile, norm_tile), norm_tile)
        value = part[mine, :].astype(jnp.float32)
        for k in range(tp - 1):
            value = value + arrived[k, here, :].astype(jnp.float32)
        layer[here, :] = value.astype(jnp.bfloat16)

    copies[2].start()
    for copy in copies:
        copy.wait()


def on_device(prompt_rows, up_master, down_master, norm_gain):
    n = lax.axis_size("fs")
    tp = lax.axis_size("tp")
    bf16 = jnp.bfloat16
    up_rows, width = up_master.shape
    span = width // n
    fs_per_tp = n // tp
    up_width = fs_per_tp * span
    down_width = down_master.shape[1]
    if fs_per_tp > 1:
        up_master = up_master.reshape(up_rows, fs_per_tp, tp, span).swapaxes(1, 2)
        up_master = up_master.reshape(up_rows, width)
    groups = column_groups(tp, (up_width, down_width))
    count = len(groups)
    tokens, model = prompt_rows.shape
    units = n * span
    share = tokens // tp
    vmem = pl.BlockSpec(memory_space=pltpu.VMEM)
    hbm = pl.BlockSpec(memory_space=pl.ANY)
    dma = pltpu.SemaphoreType.DMA
    held = pl.pallas_call(
        functools.partial(gather_kernel, n, tp, groups),
        out_shape=(
            pltpu.VMEM((model, units), bf16),
            pltpu.VMEM((units, model), bf16),
            pltpu.VMEM((tokens, model), bf16),
            pltpu.VMEM((tp - 1, share, model), bf16),
        ),
        in_specs=[hbm, hbm, vmem, hbm],
        out_specs=(vmem, vmem, vmem, vmem),
        scratch_shapes=[
            pltpu.VMEM((tokens, model), bf16),
            pltpu.VMEM((tokens, units), bf16),
            pltpu.VMEM((tokens, groups[-1][3]), jnp.float32),
            pltpu.VMEM(up_master.shape, jnp.float32),
            pltpu.VMEM(down_master.shape, jnp.float32),
            pltpu.VMEM(up_master.shape, bf16),
            pltpu.VMEM(down_master.shape, bf16),
            pltpu.VMEM((up_rows, 128), jnp.float32),
            dma((tp + 3,)),
            dma((2,)),
            dma((2, tp - 1, 2)),
            dma((3,)),
            dma((count, n - 1)),
            dma((1,)),
            dma((count + pieces * n,)),
            dma((1,)),
            dma((1,)),
        ],
        compiler_params=pltpu.CompilerParams(
            collective_id=0, has_side_effects=True, vmem_limit_bytes=32 * 1024 * 1024
        ),
    )(up_master, down_master, norm_gain[None, :], prompt_rows)
    up_sampler, down_sampler, layer_out = pl.pallas_call(
        functools.partial(place_kernel, tp),
        out_shape=(
            jax.ShapeDtypeStruct((model, units), bf16),
            jax.ShapeDtypeStruct((units, model), bf16),
            jax.ShapeDtypeStruct((share, model), bf16),
        ),
        in_specs=[vmem] * 4,
        out_specs=(hbm, hbm, hbm),
        scratch_shapes=[pltpu.VMEM((share, model), bf16), dma((3,))],
        compiler_params=pltpu.CompilerParams(vmem_limit_bytes=8 * 1024 * 1024),
    )(*held)
    return (up_sampler[None], down_sampler[None], layer_out)


def solution(mesh):
    in_specs = (P(("grp", "fs"), None), P("fs", "tp"), P("fs", "tp"), P("fs"))
    out_specs = (
        P(("grp", "tp"), None, None),
        P(("grp", "tp"), None, None),
        P(("grp", "fs", "tp"), None),
    )
    return jax.shard_map(
        on_device, mesh=mesh, in_specs=in_specs, out_specs=out_specs, check_vma=False
    )
```

time: 181 us -> 164 us (0.906)
  Pallas kernels: 180 us -> 163 us
    pallas_call x2, Pallas kernels: 180 us -> 163 us  [the longest x1 157 us: on_device(): pl.pallas_call(functools.partial(gather_kernel, n, tp, groups), out_shape...]
where the time goes in v1:
time: 164 us
  Pallas kernels  163 us (99%)
    pallas_call x1, Pallas kernels, on_device(): pl.pallas_call(functools.partial(gather_kernel, n, tp, groups), out_shape...  157 us
    pallas_call x1, Pallas kernels, on_device(): pl.pallas_call(functools.partial(place_kernel, tp), out_shape=(jax.ShapeD...  6.28 us

profile of v1, /device:TPU:1, one launch (start us, length us, event | category | flops | bytes accessed | tf_op | source)
XLA Modules:
  0.0 163.8 jit_solution(9143580682185447136)
XLA Ops:
  0.6 156.7 %shard_map.67 = (bf16[2048,2048]{1,0:T(8,128)(2,1)S(1)}, bf16[2048,2048]{1,0:T(8,128)(2,1)S(1)}, bf16[1024,2048]{1,0:T(8,128)(2,1)S(1)}, bf16[3,256,2048]{2,1,0:T(8,128)(2,1)S(1)}) custom-call(f32[512,2048]{1,0:T(8,128)} %up_ref.1, f32[2048,512]{1,0:T(8,128)} %down_ref.1, f32[1,512]{1,0:T(1,128)} %bitcast.3, bf16[1024,2048]{1,0:T(8,128)(2,1)} %rows_ref.1), custom_call_target="tpu_custom_call" | custom-call | tf_op jit(solution)/shard_map/pallas_call | solution.py:479
  157.4 6.3 %shard_map.68 = (bf16[2048,2048]{1,0:T(8,128)(2,1)}, bf16[2048,2048]{1,0:T(8,128)(2,1)}, bf16[256,2048]{1,0:T(8,128)(2,1)}) custom-call(bf16[2048,2048]{1,0:T(8,128)(2,1)S(1)} %get-tuple-element.10.up_in, bf16[2048,2048]{1,0:T(8,128)(2,1)S(1)} %get-tuple-element.11.down_in, bf16[1024,2048]{1,0:T(8,128)(2,1)S(1)} %get-tuple-element.12.part, ...), custom_call_target="tpu_custom_call" | custom-call | tf_op jit(solution)/shard_map/pallas_call | solution.py:512

commit v2 on v1

--- a/solution.py
+++ b/solution.py
@@ -9,7 +9,7 @@
 from jax.sharding import PartitionSpec as P
 
 eps = 1e-06
-row_tile = 256
+row_tile = 1024
 norm_tile = 64
 pieces = 2
 MESH = pl.DeviceIdType.MESH
@@ -313,6 +313,8 @@
         ref = alls[w].at[pl.ds(0, (n - 1) * half), columns(g, source(me, groups[g][1]))]
         remote(ref, ref, y_send.at[0], y_recv.at[g], {"grp": 1 - y}).wait_recv()
 
+    tile = math.gcd(tokens, row_tile)
+
     def finish(g):
         w, j, _, width = groups[g]
         cols = columns(g, source(me, j))
@@ -320,15 +322,15 @@
         def product(a, fresh):
             deep = pl.ds(pl.multiple_of(a * depths[1], depths[1]), depths[1])
 
-            @pl.loop(0, tokens // row_tile)
+            @pl.loop(0, tokens // tile)
             def _(m):
-                here = pl.ds(pl.multiple_of(m * row_tile, row_tile), row_tile)
+                here = pl.ds(pl.multiple_of(m * tile, tile), tile)
                 acc = jnp.dot(hidden[here, deep], down_all[deep, cols], preferred_element_type=jnp.float32)
                 total[here, :] = acc if fresh else total[here, :] + acc
 
         if in_pieces(g):
             product(z, True)
-            for s in range(1, n):
+            for s in [*range(2, n), 1]:
                 for a in range(n):
                     if a - s < 0 and a + s > n - 1:
                         continue
@@ -341,16 +343,16 @@
                         other_half(g, a)
                         product(a, False)
 
-            @pl.loop(0, tokens // row_tile)
+            @pl.loop(0, tokens // tile)
             def _(m):
-                here = pl.ds(pl.multiple_of(m * row_tile, row_tile), row_tile)
+                here = pl.ds(pl.multiple_of(m * tile, tile), tile)
                 part[here, cols] = total[here, :].astype(jnp.bfloat16)
         else:
             other_halves(g)
 
-            @pl.loop(0, tokens // row_tile)
+            @pl.loop(0, tokens // tile)
             def _(m):
-                here = pl.ds(pl.multiple_of(m * row_tile, row_tile), row_tile)
+                here = pl.ds(pl.multiple_of(m * tile, tile), tile)
                 if w == 0:
                     acc = jnp.dot(normed[here, :], up_all[:, cols], preferred_element_type=jnp.float32)
                     acc = jnp.maximum(acc, 0.0)

time: 164 us -> 160 us (0.976)
  Pallas kernels: 163 us -> 159 us
    pallas_call x1, Pallas kernels: 157 us -> 153 us  [on_device(): pl.pallas_call(functools.partial(gather_kernel, n, tp, groups), out_shape...]
where the time goes in v2:
time: 160 us
  Pallas kernels  159 us (99%)
    pallas_call x1, Pallas kernels, on_device(): pl.pallas_call(functools.partial(gather_kernel, n, tp, groups), out_shape...  153 us
    pallas_call x1, Pallas kernels, on_device(): pl.pallas_call(functools.partial(place_kernel, tp), out_shape=(jax.ShapeD...  6.28 us

profile of v2, /device:TPU:1, one launch (start us, length us, event | category | flops | bytes accessed | tf_op | source)
XLA Modules:
  0.0 159.9 jit_solution(17645964637686774679)
XLA Ops:
  0.6 152.8 %shard_map.67 = (bf16[2048,2048]{1,0:T(8,128)(2,1)S(1)}, bf16[2048,2048]{1,0:T(8,128)(2,1)S(1)}, bf16[1024,2048]{1,0:T(8,128)(2,1)S(1)}, bf16[3,256,2048]{2,1,0:T(8,128)(2,1)S(1)}) custom-call(f32[512,2048]{1,0:T(8,128)} %up_ref.1, f32[2048,512]{1,0:T(8,128)} %down_ref.1, f32[1,512]{1,0:T(1,128)} %bitcast.3, bf16[1024,2048]{1,0:T(8,128)(2,1)} %rows_ref.1), custom_call_target="tpu_custom_call" | custom-call | tf_op jit(solution)/shard_map/pallas_call | solution.py:481
  153.5 6.3 %shard_map.68 = (bf16[2048,2048]{1,0:T(8,128)(2,1)}, bf16[2048,2048]{1,0:T(8,128)(2,1)}, bf16[256,2048]{1,0:T(8,128)(2,1)}) custom-call(bf16[2048,2048]{1,0:T(8,128)(2,1)S(1)} %get-tuple-element.10.up_in, bf16[2048,2048]{1,0:T(8,128)(2,1)S(1)} %get-tuple-element.11.down_in, bf16[1024,2048]{1,0:T(8,128)(2,1)S(1)} %get-tuple-element.12.part, ...), custom_call_target="tpu_custom_call" | custom-call | tf_op jit(solution)/shard_map/pallas_call | solution.py:514

commit v3 on v2

--- a/solution.py
+++ b/solution.py
@@ -10,8 +10,10 @@
 
 eps = 1e-06
 row_tile = 1024
+step_rows = 512
 norm_tile = 64
-pieces = 2
+pieces = 4
+final_twins = 2
 MESH = pl.DeviceIdType.MESH
 
 
@@ -58,10 +60,13 @@
     widths = (up_ref.shape[1] // tp, down_ref.shape[1])
     alls = (up_all, down_all)
     tokens = rows_ref.shape[0]
+    model = down_all.shape[1]
     share = tokens // tp
     count = len(groups)
     first_down = sum(group[0] == 0 for group in groups)
     twins = n > 2
+    doubled = range(count - final_twins, count) if twins and depths[1] % 128 == 0 else range(0)
+    spare = sum(groups[g][3] for g in doubled)
     lag = max(n - 2, 2)
     steps = count + lag
     ahead, lead = 2, 3
@@ -120,6 +125,9 @@
     def half_sem(g, a):
         return y_recv.at[count + (g - count + pieces) * n + a if in_pieces(g) else g]
 
+    def half_sent(g):
+        return y_send.at[2 if g in doubled else groups[g][0]]
+
     def z_copy(g, a, way, device):
         ref = block(g, a, y)
         slot = lax.rem(a - device + n, n) - 1
@@ -131,13 +139,13 @@
     def own_down(g):
         return z_copy(g, z, 1, z - 1)
 
-    def twin_copy(g, a, device):
+    def twin_copy(g, a, way, device):
         ref = block(g, a, 1 - y)
-        return remote(ref, ref, z_send.at[2], half_sem(g, a), {"fs": device})
+        return remote(ref, ref, z_send.at[way], half_sem(g, a), {"fs": device})
 
     def y_copy(g, a, h):
         ref = block(g, a, h)
-        return remote(ref, ref, y_send.at[0], half_sem(g, a), {"grp": 1 - y})
+        return remote(ref, ref, half_sent(g), half_sem(g, a), {"grp": 1 - y})
 
     def sum_copy(g, k):
         t = target(k)
@@ -220,10 +228,14 @@
         @pl.when(z == 1)
         def _():
             own_down(g).start()
+            if g in doubled:
+                twin_copy(g, 1, 3, 0).start()
 
         @pl.when(z == n - 2)
         def _():
             own_up(g).start()
+            if g in doubled:
+                twin_copy(g, n - 2, 3 if n > 3 else 4, n - 1).start()
 
     def early_own(g):
         w, j, first, _ = groups[g]
@@ -247,7 +259,7 @@
 
                 @pl.when(z == edge)
                 def _():
-                    twin_copy(g, edge, near).start()
+                    twin_copy(g, edge, 2, near).start()
 
     def at_edge(body):
         for edge, way in ((0, 1), (n - 1, -1)):
@@ -256,9 +268,17 @@
             def _():
                 body(lambda s: edge + way * s)
 
-    def edge_receive(g, a):
+    def edge_receive(g, a, whole=False):
         z_copy(g, a, 0, z).wait_recv()
-        y_copy(g, a, y).start()
+        if not whole:
+            y_copy(g, a, y).start()
+
+    def receive_near(step):
+        def edge(at):
+            for g in plan[step]:
+                edge_receive(g, at(1), g in doubled)
+
+        at_edge(edge)
 
     def receive(step):
         @pl.when(middle)
@@ -299,8 +319,6 @@
                 g = step - (s - 2)
                 if 0 <= g < count:
                     edge_receive(g, at(s))
-            for g in plan[step]:
-                edge_receive(g, at(1))
 
         at_edge(edge)
 
@@ -311,9 +329,10 @@
         w = groups[g][0]
         half = depths[w] // 2
         ref = alls[w].at[pl.ds(0, (n - 1) * half), columns(g, source(me, groups[g][1]))]
-        remote(ref, ref, y_send.at[0], y_recv.at[g], {"grp": 1 - y}).wait_recv()
+        remote(ref, ref, half_sent(g), y_recv.at[g], {"grp": 1 - y}).wait_recv()
 
     tile = math.gcd(tokens, row_tile)
+    step_tile = math.gcd(tokens, step_rows)
 
     def finish(g):
         w, j, _, width = groups[g]
@@ -330,18 +349,13 @@
 
         if in_pieces(g):
             product(z, True)
-            for s in [*range(2, n), 1]:
-                for a in range(n):
-                    if a - s < 0 and a + s > n - 1:
-                        continue
-                    near = z - a == s if a + s < n else a - z == s
-                    if a + s < n and a - s >= 0:
-                        near = jnp.logical_or(z - a == s, a - z == s)
-
-                    @pl.when(near)
-                    def _():
-                        other_half(g, a)
-                        product(a, False)
+
+            @pl.loop(1, n)
+            def _(i):
+                turn = jnp.where(i == n - 1, 1, i + 1)
+                a = lax.rem(jnp.where(2 * z < n, z + turn, z - turn + n), n)
+                other_half(g, a)
+                product(a, False)
 
             @pl.loop(0, tokens // tile)
             def _(m):
@@ -350,9 +364,9 @@
         else:
             other_halves(g)
 
-            @pl.loop(0, tokens // tile)
+            @pl.loop(0, tokens // step_tile)
             def _(m):
-                here = pl.ds(pl.multiple_of(m * tile, tile), tile)
+                here = pl.ds(pl.multiple_of(m * step_tile, step_tile), step_tile)
                 if w == 0:
                     acc = jnp.dot(normed[here, :], up_all[:, cols], preferred_element_type=jnp.float32)
                     acc = jnp.maximum(acc, 0.0)
@@ -397,6 +411,8 @@
     sent = ahead
     for step in range(steps):
         receive(step)
+        if step < first_down + lag:
+            receive_near(step)
         while sent < count and sent <= step + lead:
             early_own(sent)
             sent += 1
@@ -410,26 +426,40 @@
             while work:
                 work.pop(0)()
             finish(step - lag)
+        if step >= first_down + lag:
+            receive_near(step)
 
     def await_sends(ref, sem):
         remote(ref, ref, sem, sum_recv.at[0], {"grp": 1 - y}).wait_send()
 
     await_sends(up_cast.at[:, pl.ds(0, (tp - 1) * widths[0])], tp_send.at[0])
     await_sends(down_cast.at[pl.ds(0, (tp - 1) * depths[1]), :], tp_send.at[1])
-    for edge in range(n):
-        passed = n - 1 - (twins and edge == 1) - (twins and edge == n - 2)
-        waits = [
-            (z_send.at[0], edge + 1 if edge < n - 1 else 0),
-            (z_send.at[1], n - edge if edge > 0 else 0),
-            (z_send.at[2], int(twins and edge in (0, n - 1))),
-            (y_send.at[0], passed),
-        ]
-
-        @pl.when(z == edge)
+    halves = [depth // 2 for depth in depths]
+    for at in range(n):
+        passed = n - 1 - (twins and at == 1) - (twins and at == n - 2)
+        up_blocks = at + 1 if at < n - 1 else 0
+        down_blocks = n - at if at > 0 else 0
+        unequal = passed - (at in (0, n - 1))
+
+        @pl.when(z == at)
         def _():
-            for sem, blocks in waits:
-                if blocks:
-                    await_sends(up_all.at[pl.ds(0, blocks * depths[0]), :], sem)
+            if up_blocks:
+                await_sends(up_all.at[pl.ds(0, up_blocks * depths[0]), :], z_send.at[0])
+            if down_blocks:
+                await_sends(up_all.at[pl.ds(0, down_blocks * depths[0]), :], z_send.at[1])
+            if twins and at in (0, n - 1):
+                await_sends(up_all.at[pl.ds(0, depths[0]), :], z_send.at[2])
+            if spare and at == 1:
+                await_sends(down_all.at[pl.ds(0, halves[1]), pl.ds(0, spare)], z_send.at[3])
+            if spare and at == n - 2:
+                way = 3 if n > 3 else 4
+                await_sends(down_all.at[pl.ds(0, halves[1]), pl.ds(0, spare)], z_send.at[way])
+            if passed:
+                await_sends(up_all.at[pl.ds(0, passed * halves[0]), :], y_send.at[0])
+                rest = pl.ds(0, model - spare)
+                await_sends(down_all.at[pl.ds(0, passed * halves[1]), rest], y_send.at[1])
+            if spare and unequal:
+                await_sends(down_all.at[pl.ds(0, unequal * halves[1]), pl.ds(0, spare)], y_send.at[2])
 
     remote(arrived, arrived, sum_send.at[0], sum_recv.at[0], {"grp": 1 - y}).wait()
 
@@ -500,9 +530,9 @@
             dma((tp + 3,)),
             dma((2,)),
             dma((2, tp - 1, 2)),
+            dma((5,)),
+            dma((count, n - 1)),
             dma((3,)),
-            dma((count, n - 1)),
-            dma((1,)),
             dma((count + pieces * n,)),
             dma((1,)),
             dma((1,)),

time: 160 us -> 159 us (level)
  no operation moved by 1% of the time
where the time goes in v3:
time: 159 us
  Pallas kernels  158 us (99%)
    pallas_call x1, Pallas kernels, on_device(): pl.pallas_call(functools.partial(gather_kernel, n, tp, groups), out_shape...  152 us
    pallas_call x1, Pallas kernels, on_device(): pl.pallas_call(functools.partial(place_kernel, tp), out_shape=(jax.ShapeD...  6.28 us

profile of v3, /device:TPU:1, one launch (start us, length us, event | category | flops | bytes accessed | tf_op | source)
XLA Modules:
  0.0 158.7 jit_solution(17843484073105811651)
XLA Ops:
  0.6 151.6 %shard_map.67 = (bf16[2048,2048]{1,0:T(8,128)(2,1)S(1)}, bf16[2048,2048]{1,0:T(8,128)(2,1)S(1)}, bf16[1024,2048]{1,0:T(8,128)(2,1)S(1)}, bf16[3,256,2048]{2,1,0:T(8,128)(2,1)S(1)}) custom-call(f32[512,2048]{1,0:T(8,128)} %up_ref.1, f32[2048,512]{1,0:T(8,128)} %down_ref.1, f32[1,512]{1,0:T(1,128)} %bitcast.3, bf16[1024,2048]{1,0:T(8,128)(2,1)} %rows_ref.1), custom_call_target="tpu_custom_call" | custom-call | tf_op jit(solution)/shard_map/pallas_call | solution.py:511
  152.2 6.3 %shard_map.68 = (bf16[2048,2048]{1,0:T(8,128)(2,1)}, bf16[2048,2048]{1,0:T(8,128)(2,1)}, bf16[256,2048]{1,0:T(8,128)(2,1)}) custom-call(bf16[2048,2048]{1,0:T(8,128)(2,1)S(1)} %get-tuple-element.10.up_in, bf16[2048,2048]{1,0:T(8,128)(2,1)S(1)} %get-tuple-element.11.down_in, bf16[1024,2048]{1,0:T(8,128)(2,1)S(1)} %get-tuple-element.12.part, ...), custom_call_target="tpu_custom_call" | custom-call | tf_op jit(solution)/shard_map/pallas_call | solution.py:544

commit v4 on v3

--- a/solution.py
+++ b/solution.py
@@ -10,7 +10,7 @@
 
 eps = 1e-06
 row_tile = 1024
-step_rows = 512
+step_rows = 256
 norm_tile = 64
 pieces = 4
 final_twins = 2
@@ -350,17 +350,24 @@
         if in_pieces(g):
             product(z, True)
 
-            @pl.loop(1, n)
+            def partner(turn):
+                return lax.rem(jnp.where(2 * z < n, z + turn, z - turn + n), n)
+
+            @pl.loop(1, n - 1)
             def _(i):
-                turn = jnp.where(i == n - 1, 1, i + 1)
-                a = lax.rem(jnp.where(2 * z < n, z + turn, z - turn + n), n)
+                a = partner(i + 1)
                 other_half(g, a)
                 product(a, False)
+
+            last = partner(1)
+            other_half(g, last)
+            deep = pl.ds(pl.multiple_of(last * depths[1], depths[1]), depths[1])
 
             @pl.loop(0, tokens // tile)
             def _(m):
                 here = pl.ds(pl.multiple_of(m * tile, tile), tile)
-                part[here, cols] = total[here, :].astype(jnp.bfloat16)
+                acc = jnp.dot(hidden[here, deep], down_all[deep, cols], preferred_element_type=jnp.float32)
+                part[here, cols] = (total[here, :] + acc).astype(jnp.bfloat16)
         else:
             other_halves(g)
 

time: 159 us -> 159 us (level)
  no operation moved by 1% of the time
where the time goes in v4:
time: 159 us
  Pallas kernels  158 us (99%)
    pallas_call x1, Pallas kernels, on_device(): pl.pallas_call(functools.partial(gather_kernel, n, tp, groups), out_shape...  152 us
    pallas_call x1, Pallas kernels, on_device(): pl.pallas_call(functools.partial(place_kernel, tp), out_shape=(jax.ShapeD...  6.28 us

profile of v4, /device:TPU:1, one launch (start us, length us, event | category | flops | bytes accessed | tf_op | source)
XLA Modules:
  0.0 159.2 jit_solution(4060928323827055021)
XLA Ops:
  0.6 152.1 %shard_map.67 = (bf16[2048,2048]{1,0:T(8,128)(2,1)S(1)}, bf16[2048,2048]{1,0:T(8,128)(2,1)S(1)}, bf16[1024,2048]{1,0:T(8,128)(2,1)S(1)}, bf16[3,256,2048]{2,1,0:T(8,128)(2,1)S(1)}) custom-call(f32[512,2048]{1,0:T(8,128)} %up_ref.1, f32[2048,512]{1,0:T(8,128)} %down_ref.1, f32[1,512]{1,0:T(1,128)} %bitcast.3, bf16[1024,2048]{1,0:T(8,128)(2,1)} %rows_ref.1), custom_call_target="tpu_custom_call" | custom-call | tf_op jit(solution)/shard_map/pallas_call | solution.py:518
  152.8 6.3 %shard_map.68 = (bf16[2048,2048]{1,0:T(8,128)(2,1)}, bf16[2048,2048]{1,0:T(8,128)(2,1)}, bf16[256,2048]{1,0:T(8,128)(2,1)}) custom-call(bf16[2048,2048]{1,0:T(8,128)(2,1)S(1)} %get-tuple-element.10.up_in, bf16[2048,2048]{1,0:T(8,128)(2,1)S(1)} %get-tuple-element.11.down_in, bf16[1024,2048]{1,0:T(8,128)(2,1)S(1)} %get-tuple-element.12.part, ...), custom_call_target="tpu_custom_call" | custom-call | tf_op jit(solution)/shard_map/pallas_call | solution.py:551
